TPU v7x, 32 devices: a whole 2x2x4 slice. The times are simulated.
32 devices in a mesh: ep: 8 (over z, x), tp: 4 (over y, core).
Axes of the slice: x: 2, y: 2, z: 4, core: 2. Of those that a mesh axis runs over, the one named last changes fastest.
Arguments:
- tokens: bfloat16 [192, 3072], P('ep'), may hold values from -6 to 6
- norm_gain: float32 [3072], replicated, may hold values from 0.1 to 1.9
- routing: int32 [192, 4], P('ep'), may hold values from 0 to 7, all different within a row; in each aligned block of 24 rows (0 to 23, 24 to 47, ...) at most 13 rows name the same one
- route_weight: float32 [192, 4], P('ep'), may hold values from 0.05 to 1
- w_gate: bfloat16 [8, 3072, 3072], P('ep', None, 'tp'), may hold values from -0.3125 to 0.3125
- w_up: bfloat16 [8, 3072, 3072], P('ep', None, 'tp'), may hold values from -0.3125 to 0.3125
- w_down: bfloat16 [8, 3072, 3072], P('ep', 'tp'), may hold values from -0.01953125 to 0.01953125
Outputs:
- mixed: bfloat16 [192, 3072], P('ep', 'tp')
Inputs may be any that keep to these rules, and one draw needn't show every extreme that they name: `routing`: each row names 4 different experts. Within the rows of one device (aligned blocks of 24 rows) no expert is named by more than 13 rows, a bound that some block reaches.
All inputs are finite; a program needn't handle non-finite values.
Results may differ from a plain program's by a relative error of at most 0.019.
Values may be sent and summed in bfloat16 or wider, within the bound.
A program may use at most 64 MiB of HBM per device.

v0:
```python
import jax
import jax.numpy as jnp
from jax import lax
from jax.sharding import PartitionSpec as P

NORM_EPS = 1e-06
CLAMP_LIMIT = 7.0
SIGMOID_SCALE = 1.702


def slot_index(route_rows, expert_total, capacity):
    flat_ids = route_rows.reshape(-1)
    one_hot = (flat_ids[:, None] == jnp.arange(expert_total, dtype=jnp.int32)[None, :]).astype(
        jnp.int32
    )
    before = jnp.cumsum(one_hot, axis=0) - one_hot
    ranked = jnp.sum(before * one_hot, axis=1)
    return flat_ids * capacity + ranked


def local(tokens, norm_gain, routing, route_weight, w_gate, w_up, w_down):
    tok_count = tokens.shape[0]
    width = tokens.shape[1]
    top_count = routing.shape[1]
    expert_total = lax.axis_size("ep") * w_gate.shape[0]
    capacity = max(2, tok_count * top_count // expert_total + 1)
    slice_width = width // lax.axis_size("tp")
    values = tokens.astype(jnp.float32)
    scaled = values * lax.rsqrt(jnp.mean(values * values, axis=-1, keepdims=True) + NORM_EPS)
    normal = (scaled * norm_gain).astype(jnp.bfloat16)
    dest = slot_index(routing, expert_total, capacity)
    slot_ids = jnp.arange(expert_total * capacity, dtype=jnp.int32)
    select = jnp.sum(dest.reshape(1, tok_count, top_count) == slot_ids[:, None, None], axis=2)
    sending = jnp.dot(
        select.astype(jnp.bfloat16), normal, preferred_element_type=jnp.float32
    ).astype(jnp.bfloat16)
    gate_mat = w_gate[0]
    up_mat = w_up[0]
    down_mat = w_down[0]
    own_share = lax.dynamic_slice_in_dim(
        sending, lax.axis_index("tp") * slice_width, slice_width, 1
    )
    arrived = lax.all_to_all(own_share, "ep", split_axis=0, concat_axis=0, tiled=True)
    pieces = lax.all_gather(arrived, "tp", axis=1, tiled=True)
    gate_pre = jnp.dot(pieces, gate_mat, preferred_element_type=jnp.float32)
    up_pre = jnp.dot(pieces, up_mat, preferred_element_type=jnp.float32)
    gated = jnp.minimum(gate_pre, CLAMP_LIMIT)
    upper = jnp.clip(up_pre, -CLAMP_LIMIT, CLAMP_LIMIT)
    hidden = ((upper + 1.0) * gated * jax.nn.sigmoid(SIGMOID_SCALE * gated)).astype(jnp.bfloat16)
    summed = lax.psum_scatter(
        lax.dot_general(
            down_mat, hidden, (((0,), (1,)), ((), ())), preferred_element_type=jnp.float32
        ).astype(jnp.bfloat16),
        "tp",
        scatter_dimension=0,
        tiled=True,
    )
    back = lax.all_to_all(summed, "ep", split_axis=1, concat_axis=1, tiled=True)
    picked = back[:, dest].reshape(slice_width, tok_count, top_count)
    mixed = jnp.sum(picked.astype(jnp.float32) * route_weight[None, :, :], axis=2)
    return mixed.T.astype(jnp.bfloat16)


def solution(mesh):
    placed = (
        P("ep", None),
        P(),
        P("ep", None),
        P("ep", None),
        P("ep", None, "tp"),
        P("ep", None, "tp"),
        P("ep", "tp", None),
    )
    return jax.shard_map(
        local, mesh=mesh, in_specs=placed, out_specs=P("ep", "tp"), check_vma=False
    )
```

profile of v0, /device:TPU:0, one launch (start us, length us, event | category | flops | bytes accessed | tf_op | source)
XLA Modules:
  0.0 87.3 jit_solution(828306079801427838)
XLA Ops:
  6.5 0.0 reduce-scatter.2.cloned.1.call-start
  6.5 0.8 copy.14
  7.3 0.1 eq.28
  7.4 0.1 fusion.48
  7.5 0.1 reduce_window_sum.11
  7.6 0.2 select_reduce_fusion
  7.8 0.1 reduce_sum.41
  7.9 0.1 copy.16
  8.0 0.1 convert_reduce_fusion
  8.1 1.0 %fusion.37 = f32[24]{0:T(128)S(1)} fusion(bf16[24,3072]{1,0:T(8,128)(2,1)} %param.7), kind=kLoop, calls=%fused_computation.23 | loop fusion | flops 221160 | bytes 147552 | tf_op jit(solution)/shard_map/reduce_sum | solution.py:29
  9.2 1.3 %fusion.44 = bf16[104,3072]{1,0:T(8,128)(2,1)S(1)} fusion(bf16[24,3072]{1,0:T(8,128)(2,1)} %param.7, f32[3072]{0:T(1024)} %param.8, f32[24]{0:T(128)S(1)} %add_rsqrt_fusion, s32[104,24]{0,1:T(8,128)S(1)} %convert_reduce_fusion), kind=kOutput, calls=%fused_computation.32 | convolution fusion | flops 15632832 | bytes 808800 | tf_op jit(solution)/shard_map/dot_general | solution.py:34
  10.5 0.1 all_to_all.16
  10.6 15.0 %all_to_all.24 = bf16[8,13,768]{2,1,0:T(8,128)(2,1)S(1)} all-to-all(bf16[8,13,768]{2,1,0:T(8,128)(2,1)S(1)} %all_to_all.16), channel_id=1, replica_groups=mesh['ep'=8,'tp'=4] {'ep'}, dimensions={0} | all-to-all | bytes 319488 | tf_op jit(solution)/shard_map/all_to_all | solution.py:43
  25.6 0.1 all_to_all.18
  25.7 7.8 %all_gather.3 = bf16[104,3072]{1,0:T(8,128)(2,1)S(1)} all-gather(bf16[104,768]{1,0:T(8,128)(2,1)S(1)} %all_to_all.18), channel_id=1, replica_groups=mesh['ep'=8,'tp'=4] {'tp'}, dimensions={1}, use_global_device_ids=true | all-gather | bytes 798720 | tf_op jit(solution)/shard_map/all_gather | solution.py:44
  33.5 3.2 %fusion.12 = f32[104,768]{1,0:T(8,128)S(1)} fusion(bf16[104,3072]{1,0:T(8,128)(2,1)S(1)} %all_gather.3, bf16[1,3072,768]{2,1,0:T(8,128)(2,1)} %param.11), kind=kOutput, calls=%fused_computation.9 | convolution fusion | flops 490813440 | bytes 5677056 | tf_op jit(solution)/shard_map/dot_general | solution.py:45
  36.7 0.0 copy-start
  36.7 6.5 %fusion.9 = bf16[3072,104]{0,1:T(8,128)(2,1)} fusion(bf16[1,768,3072]{2,1,0:T(8,128)(2,1)} %param.13, f32[104,768]{1,0:T(8,128)S(1)} %fusion.12, bf16[104,3072]{1,0:T(8,128)(2,1)S(1)} %all_gather.3, bf16[1,3072,768]{2,1,0:T(8,128)(2,1)} %param.12), kind=kOutput, calls=%fused_computation.8 | convolution fusion | flops 982505472 | bytes 11034624 | tf_op jit(solution)/shard_map/dot_general | solution.py:51
  43.2 0.0 reduce-scatter.2.cloned.1.call-update
  43.2 0.1 mul.76
  43.3 0.0 copy-done
  43.4 0.1 copy.17
  43.4 20.2 %reduce-scatter.2.cloned.1.call-done = bf16[768,104]{0,1:T(8,128)(2,1)} async-done(((bf16[3072,104]{0,1:T(8,128)(2,1)}), bf16[768,104]{0,1:T(8,128)(2,1)}) %reduce-scatter.2.cloned.1.call-update) | async-done | bytes 159760 | tf_op jit(solution)/shard_map/reduce_scatter | solution.py:50
  63.7 1.6 %all_to_all.19 = bf16[768,8,13]{0,2,1:T(8,128)(2,1)} reshape(bf16[768,104]{0,1:T(8,128)(2,1)} %reduce-scatter.2.cloned.1.call-done) | data formatting | bytes 319488 | tf_op jit(solution)/shard_map/all_to_all | solution.py:58
  65.3 5.5 %all-to-all-start.1 = ((bf16[768,8,13]{0,2,1:T(8,128)(2,1)}), bf16[768,8,13]{0,2,1:T(8,128)(2,1)S(1)}, u32[]{:S(2)}, u32[]{:S(2)}) async-start(bf16[768,8,13]{0,2,1:T(8,128)(2,1)} %all_to_all.19), calls=%async_computation.2 | async-start | bytes 393216 | tf_op jit(solution)/shard_map/all_to_all | solution.py:58
  70.8 7.8 %all-to-all-done.1 = bf16[768,8,13]{0,2,1:T(8,128)(2,1)S(1)} async-done(((bf16[768,8,13]{0,2,1:T(8,128)(2,1)}), bf16[768,8,13]{0,2,1:T(8,128)(2,1)S(1)}, u32[]{:S(2)}, u32[]{:S(2)}) %all-to-all-start.1) | async-done | bytes 159776 | tf_op jit(solution)/shard_map/all_to_all | solution.py:58
  78.6 0.1 all_to_all.21
  78.7 0.8 gather_fusion
  79.5 0.1 reshape.54
  79.6 0.9 multiply_reduce_fusion
  (6 shorter events, 0.1 us)
Async XLA Ops:
  6.5 57.1 %reduce-scatter.2.cloned.1.call-start = ((), (), s32[]{:S(2)}) async-start(), calls=%async_computation.3 | async-start | bytes 798720 | tf_op jit(solution)/shard_map/reduce_scatter | solution.py:50
  36.7 6.7 %copy-start = (f32[24,4]{0,1:T(4,128)S(1)}, f32[24,4]{0,1:T(4,128)}, u32[]{:S(2)}) copy-start(f32[24,4]{0,1:T(4,128)} %param.10) | copy-start | bytes 1156
  65.3 13.3 %all-to-all-start.1 = ((bf16[768,8,13]{0,2,1:T(8,128)(2,1)}), bf16[768,8,13]{0,2,1:T(8,128)(2,1)S(1)}, u32[]{:S(2)}, u32[]{:S(2)}) async-start(bf16[768,8,13]{0,2,1:T(8,128)(2,1)} %all_to_all.19), calls=%async_computation.2 | async-start | bytes 393216 | tf_op jit(solution)/shard_map/all_to_all | solution.py:58
Sparse Core Ops, SparseCore 0:
  43.4 20.2 reduce-scatter.1
where the time goes:
time: 87.7 us; the launch traced here: 87.3 us
  waiting for transfers between devices  28 us (32%)
  blocking collectives  22.9 us (26%)
  between operations  13.5 us (15%)
  matrix products  11 us (13%)
  starting transfers between devices  5.5 us (6%)
  local copies, waits for them, and re-layouts  3.96 us (5%)
  other arithmetic  2.44 us (3%)
    reduce_scatter x1, waiting for transfers between devices, local(): lax.psum_scatter(lax.dot_general(down_mat, hidden, (((0,), (1,)), ((), ()...  20.2 us
    all_to_all x1, blocking collectives, local(): lax.all_to_all(own_share, 'ep', split_axis=0, concat_axis=0, tiled=True)  15 us
    all_gather x1, blocking collectives, local(): pieces = lax.all_gather(arrived, 'tp', axis=1, tiled=True)  7.82 us
    all_to_all x1, waiting for transfers between devices, local(): back = lax.all_to_all(summed, 'ep', split_axis=1, concat_axis=1, tiled=True)  7.77 us
    dot_general x1, matrix products, local(): lax.dot_general(down_mat, hidden, (((0,), (1,)), ((), ())), preferred_ele...  6.54 us
    all_to_all x1, starting transfers between devices, local(): back = lax.all_to_all(summed, 'ep', split_axis=1, concat_axis=1, tiled=True)  5.5 us
    dot_general x1, matrix products, local(): gate_pre = jnp.dot(pieces, gate_mat, preferred_element_type=jnp.float32)  3.18 us
  transfers between devices with their start and end apart: 2, of which 2 were waited for; matrix products, arithmetic and copies ran while one was open for 0% of the time, Pallas kernels for 0%

commit v1 on v0

v1 whole, which is shorter than its diff:
```python
import functools

import jax
import jax.numpy as jnp
from jax import lax
from jax.experimental import pallas as pl
from jax.experimental.pallas import tpu as pltpu
from jax.sharding import PartitionSpec as P

NORM_EPS = 1e-06
CLAMP_LIMIT = 7.0
SIGMOID_SCALE = 1.702
F32 = jnp.float32
BF16 = jnp.bfloat16
MESH = pl.DeviceIdType.MESH


def each(count, body):
    if count <= 8:
        for k in range(count):
            body(k)
    else:
        lax.fori_loop(0, count, lambda k, c: (body(k), c)[1], 0)


def kernel(
    n_ep, n_tp, tok_ref, gain_ref, route_ref, weight_ref, wg_hbm, wu_hbm, wd_hbm, out_ref,
    wg, wu, wd, acc_g, acc_u, sbuf, gbuf, part, din, ysend, yin, own, obuf, back,
    w_sem, a_send, a_recv, yf_send, yf_recv, cf_send, cf_recv, rl_send, rl_recv,
    d_send, d_recv, ys_send, ys_recv, b_send, b_recv,
):
    me = lax.axis_index("ep")
    j = lax.axis_index("tp")
    ny = n_tp // 2
    y, c = j // 2, j % 2
    core = y * 2 + (1 - c)
    toks, width = tok_ref.shape
    share = width // n_tp
    slot_rows = sbuf.shape[1]
    rows = n_ep * slot_rows
    top = route_ref.shape[1]
    others = [(y + d) % ny for d in range(1, ny)]
    order = [j, core] + [yy * 2 + c for yy in others] + [yy * 2 + (1 - c) for yy in others]
    aligned = share % 128 == 0

    def far(k):
        sign = 1 - 2 * (k % 2)
        return n_ep // 2 + sign * ((k + 1) // 2)

    def part_rows(s):
        start = s * share
        return pl.ds(pl.multiple_of(start, share) if not isinstance(start, int) else start, share)

    weight_copies = []
    for at, s in enumerate(order):
        cut = part_rows(s)
        pair = (
            pltpu.make_async_copy(wg_hbm.at[0, cut, :], wg.at[cut, :], w_sem.at[0, at]),
            pltpu.make_async_copy(wu_hbm.at[0, cut, :], wu.at[cut, :], w_sem.at[1, at]),
        )
        pair[0].start()
        pair[1].start()
        weight_copies.append(pair)

    down_order = []
    for yy in others + [y]:
        down_order += [yy * 2 + (1 - c), yy * 2 + c]
    down_copies = []
    if aligned:
        for at, s in enumerate(down_order):
            cut = part_rows(s)
            down_copies.append(
                pltpu.make_async_copy(wd_hbm.at[0, :, cut], wd.at[:, cut], w_sem.at[2, at])
            )
    else:
        down_copies.append(pltpu.make_async_copy(wd_hbm.at[0], wd, w_sem.at[2, 0]))
    for copy in down_copies:
        copy.start()

    barrier = pltpu.get_barrier_semaphore()

    def greet(k):
        pl.semaphore_signal(
            barrier, inc=1, device_id=((me + k + 1) % n_ep, j), device_id_type=MESH
        )

    each(n_ep - 1, greet)
    for peer in [core] + [yy * 2 + c for yy in others]:
        pl.semaphore_signal(barrier, inc=1, device_id=(me, peer), device_id_type=MESH)

    routes = route_ref[...]
    lanes = lax.broadcasted_iota(jnp.int32, (toks, 128), 1)
    chosen = jnp.zeros((toks, 128), F32)
    weights = jnp.zeros((toks, 128), F32)
    for k in range(top):
        hit = routes[:, k : k + 1] == lanes
        chosen += jnp.where(hit, 1.0, 0.0)
        weights += jnp.where(hit, weight_ref[:, k : k + 1], 0.0)
    before = lax.broadcasted_iota(jnp.int32, (toks, toks), 0) > lax.broadcasted_iota(
        jnp.int32, (toks, toks), 1
    )
    rank = jnp.dot(
        jnp.where(before, 1.0, 0.0).astype(BF16), chosen.astype(BF16), preferred_element_type=F32
    )
    r_row = lax.broadcasted_iota(jnp.int32, (rows, 128), 0)
    r_exp = lax.broadcasted_iota(jnp.int32, (rows, 128), 1)
    spread = jnp.where(r_row // slot_rows == r_exp, 1.0, 0.0).astype(BF16)
    nt = (((1,), (1,)), ((), ()))

    def across(a, b):
        return lax.dot_general(a, b, nt, preferred_element_type=F32)

    slot_a = (lax.broadcasted_iota(jnp.int32, (rows, toks), 0) % slot_rows).astype(F32)
    taken = across(spread, chosen.astype(BF16)) > 0.5
    select = jnp.where(
        taken & (across(spread, rank.astype(BF16)) == slot_a), 1.0, 0.0
    ).astype(BF16)

    values = tok_ref[...].astype(F32)
    scale = lax.rsqrt(jnp.mean(values * values, axis=-1, keepdims=True) + NORM_EPS)

    def put_share(tok_part, gain_part):
        normal = (tok_part.astype(F32) * scale * gain_part).astype(BF16)
        sending = jnp.dot(select, normal, preferred_element_type=F32).astype(BF16)
        sbuf[...] = sending.reshape(n_ep, slot_rows, share)

    if aligned:
        put_share(tok_ref[:, part_rows(j)], gain_ref[:, part_rows(j)])
    else:
        for s in range(n_tp):

            @pl.when(j == s)
            def _(s=s):
                cut = slice(s * share, (s + 1) * share)
                put_share(tok_ref[:, cut], gain_ref[:, cut])

    pl.semaphore_wait(barrier, n_ep - 1 + 1 + ny - 1)

    def a_copy(dst, src):
        return pltpu.make_async_remote_copy(
            src_ref=sbuf.at[dst], dst_ref=gbuf.at[j, src], send_sem=a_send.at[dst],
            recv_sem=a_recv.at[src], device_id=(dst, j), device_id_type=MESH,
        )

    def yf_copy(block, slot, yy, frm):
        return pltpu.make_async_remote_copy(
            src_ref=gbuf.at[slot, block], dst_ref=gbuf.at[slot, block],
            send_sem=yf_send.at[yy, block], recv_sem=yf_recv.at[frm, block],
            device_id=(me, yy * 2 + c), device_id_type=MESH,
        )

    def cf_copy(block, slot):
        return pltpu.make_async_remote_copy(
            src_ref=gbuf.at[slot, block], dst_ref=gbuf.at[slot, block],
            send_sem=cf_send.at[block], recv_sem=cf_recv.at[block],
            device_id=(me, core), device_id_type=MESH,
        )

    def rl_copy(slot, frm):
        return pltpu.make_async_remote_copy(
            src_ref=gbuf.at[slot], dst_ref=gbuf.at[slot], send_sem=rl_send.at[frm],
            recv_sem=rl_recv.at[frm], device_id=(me, core), device_id_type=MESH,
        )

    each(n_ep - 1, lambda k: a_copy((me + far(k)) % n_ep, me).start())
    gbuf[j, me] = sbuf[me]

    def forward(block):
        for yy in others:
            yf_copy(block, j, yy, y).start()
        cf_copy(block, j).start()

    forward(me)

    def arrive(k):
        src = (me + far(n_ep - 2 - k)) % n_ep
        a_copy(src, src).wait_recv()
        forward(src)

    each(n_ep - 1, arrive)

    place = across(weights.astype(BF16), spread)
    rest = weights - weights.astype(BF16).astype(F32)
    rest_place = across(rest.astype(BF16), spread)
    slot_b = (lax.broadcasted_iota(jnp.int32, (toks, rows), 1) % slot_rows).astype(F32)
    here = (across(rank.astype(BF16), spread) == slot_b) & (
        across(chosen.astype(BF16), spread) > 0.5
    )
    mix_high = jnp.where(here, place, 0.0).astype(BF16)
    mix_low = jnp.where(here, rest_place, 0.0).astype(BF16)

    def project(at):
        s = order[at]
        for copy in weight_copies[at]:
            copy.wait()
        piece = gbuf[s].reshape(rows, share)
        cut = part_rows(s)
        g = jnp.dot(piece, wg[cut, :], preferred_element_type=F32)
        u = jnp.dot(piece, wu[cut, :], preferred_element_type=F32)
        if at == 0:
            acc_g[...] = g
            acc_u[...] = u
        elif at < n_tp - 1:
            acc_g[...] += g
            acc_u[...] += u
        else:
            return acc_g[...] + g, acc_u[...] + u

    project(0)
    for yy in others:
        slot = yy * 2 + c
        each(n_ep, lambda b: yf_copy(b, slot, yy, yy).wait_recv())
        rl_copy(slot, yy).start()
    each(n_ep, lambda b: cf_copy(b, core).wait_recv())
    project(1)
    for at in range(2, 1 + ny):
        project(at)
    for at in range(1 + ny, n_tp):
        yy = others[at - 1 - ny]
        rl_copy(yy * 2 + (1 - c), yy).wait_recv()
        last = project(at)
    gate_pre, up_pre = last
    gated = jnp.minimum(gate_pre, CLAMP_LIMIT)
    upper = jnp.clip(up_pre, -CLAMP_LIMIT, CLAMP_LIMIT)
    hidden = ((upper + 1.0) * gated * jax.nn.sigmoid(SIGMOID_SCALE * gated)).astype(BF16)

    def d_copy(yy):
        return pltpu.make_async_remote_copy(
            src_ref=part.at[yy], dst_ref=din.at[yy], send_sem=d_send.at[yy],
            recv_sem=d_recv.at[yy], device_id=(me, core), device_id_type=MESH,
        )

    def ys_copy(block, yy, frm):
        return pltpu.make_async_remote_copy(
            src_ref=ysend.at[yy, block], dst_ref=yin.at[frm, block],
            send_sem=ys_send.at[yy, block], recv_sem=ys_recv.at[frm, block],
            device_id=(me, yy * 2 + c), device_id_type=MESH,
        )

    def b_copy(dst, src):
        return pltpu.make_async_remote_copy(
            src_ref=obuf.at[dst], dst_ref=back.at[src], send_sem=b_send.at[dst],
            recv_sem=b_recv.at[src], device_id=(dst, j), device_id_type=MESH,
        )

    def shaped(value):
        return value.reshape(n_ep, slot_rows, share)

    if aligned:

        def down(at):
            down_copies[at].wait()
            return jnp.dot(hidden, wd[:, part_rows(down_order[at])], preferred_element_type=F32)

        def close(done):
            d_copy(done).wait_recv()
            ysend[done] = (own[done].astype(F32) + din[done].astype(F32)).astype(BF16)
            each(n_ep, lambda k: ys_copy((me + far(k)) % n_ep, done, y).start())

        turn = others + [y]
        for i, yy in enumerate(turn):
            part[yy] = shaped(down(2 * i).astype(BF16))
            d_copy(yy).start()
            if i > 0:
                close(turn[i - 1])
            own[yy] = shaped(down(2 * i + 1).astype(BF16))
        d_copy(y).wait_recv()
    else:
        down_copies[0].wait()
        for s in range(n_tp):
            cut = slice(s * share, (s + 1) * share)
            value = shaped(jnp.dot(hidden, wd[:, cut], preferred_element_type=F32).astype(BF16))

            @pl.when(c == s % 2)
            def _(value=value, s=s):
                own[s // 2] = value

            @pl.when(c != s % 2)
            def _(value=value, s=s):
                part[s // 2] = value

        for yy in others + [y]:
            d_copy(yy).start()
        for yy in others + [y]:
            d_copy(yy).wait_recv()
            ysend[yy] = (own[yy].astype(F32) + din[yy].astype(F32)).astype(BF16)
        for yy in others:
            each(n_ep, lambda k: ys_copy((me + far(k)) % n_ep, yy, y).start())

    def finish(k):
        block = (me + far(k)) % n_ep
        total = own[y, block].astype(F32) + din[y, block].astype(F32)
        for yy in others:
            ys_copy(block, yy, yy).wait_recv()
            total += yin[yy, block].astype(F32)
        return block, total.astype(BF16)

    def finish_send(k):
        block, value = finish(k)
        obuf[block] = value
        b_copy(block, me).start()

    each(n_ep - 1, finish_send)
    _, value = finish(n_ep - 1)
    back[me] = value
    each(n_ep - 1, lambda k: b_copy((me + k + 1) % n_ep, (me + k + 1) % n_ep).wait_recv())
    returned = back[...].reshape(rows, share)
    mixed = jnp.dot(mix_high, returned, preferred_element_type=F32)
    mixed += jnp.dot(mix_low, returned, preferred_element_type=F32)
    out_ref[...] = mixed.astype(BF16)

    def drain(k):
        peer = (me + k + 1) % n_ep
        a_copy(peer, me).wait_send()
        b_copy(peer, me).wait_send()

    each(n_ep - 1, drain)

    def drain_blocks(b):
        cf_copy(b, j).wait_send()
        for yy in others:
            yf_copy(b, j, yy, y).wait_send()
            ys_copy(b, yy, y).wait_send()

    each(n_ep, drain_blocks)
    for yy in others:
        rl_copy(yy * 2 + c, yy).wait_send()
    for yy in others + [y]:
        d_copy(yy).wait_send()


def local(n_ep, n_tp, tokens, norm_gain, routing, route_weight, w_gate, w_up, w_down):
    toks, width = tokens.shape
    share = width // n_tp
    hidden = w_gate.shape[2]
    ny = n_tp // 2
    capacity = max(2, toks * routing.shape[1] // n_ep + 1)
    slot_rows = -(-capacity // 16) * 16
    rows = n_ep * slot_rows
    blocks = (n_ep, slot_rows, share)
    vmem = pl.BlockSpec(memory_space=pltpu.VMEM)
    hbm = pl.BlockSpec(memory_space=pl.ANY)
    dma = pltpu.SemaphoreType.DMA
    return pl.pallas_call(
        functools.partial(kernel, n_ep, n_tp),
        out_shape=jax.ShapeDtypeStruct((toks, share), BF16),
        in_specs=[vmem] * 4 + [hbm] * 3,
        out_specs=vmem,
        scratch_shapes=[
            pltpu.VMEM((width, hidden), BF16),
            pltpu.VMEM((width, hidden), BF16),
            pltpu.VMEM((hidden, width), BF16),
            pltpu.VMEM((rows, hidden), F32),
            pltpu.VMEM((rows, hidden), F32),
            pltpu.VMEM(blocks, BF16),
            pltpu.VMEM((n_tp,) + blocks, BF16),
            pltpu.VMEM((ny,) + blocks, BF16),
            pltpu.VMEM((ny,) + blocks, BF16),
            pltpu.VMEM((ny,) + blocks, BF16),
            pltpu.VMEM((ny,) + blocks, BF16),
            pltpu.VMEM((ny,) + blocks, BF16),
            pltpu.VMEM(blocks, BF16),
            pltpu.VMEM(blocks, BF16),
            dma((3, n_tp)),
            dma((n_ep,)), dma((n_ep,)),
            dma((ny, n_ep)), dma((ny, n_ep)),
            dma((n_ep,)), dma((n_ep,)),
            dma((ny,)), dma((ny,)),
            dma((ny,)), dma((ny,)),
            dma((ny, n_ep)), dma((ny, n_ep)),
            dma((n_ep,)), dma((n_ep,)),
        ],
        compiler_params=pltpu.CompilerParams(collective_id=0, has_side_effects=True),
    )(tokens, norm_gain.reshape(1, width), routing, route_weight, w_gate, w_up, w_down)


def solution(mesh):
    placed = (
        P("ep", None),
        P(),
        P("ep", None),
        P("ep", None),
        P("ep", None, "tp"),
        P("ep", None, "tp"),
        P("ep", "tp", None),
    )
    return jax.shard_map(
        functools.partial(local, mesh.shape["ep"], mesh.shape["tp"]),
        mesh=mesh, in_specs=placed, out_specs=P("ep", "tp"), check_vma=False,
    )
```

time: 87.7 us -> 36.3 us (0.41)
  Pallas kernels: 0 us -> 31.9 us
  waiting for transfers between devices: 28 us -> 0 us
  blocking collectives: 22.9 us -> 0 us
  between operations: 13.5 us -> 0.01 us
  matrix products: 11 us -> 0 us
  starting transfers between devices: 5.5 us -> 0 us
  other arithmetic: 2.44 us -> 0 us
    pallas_call x0 -> x1, Pallas kernels: none -> 31.9 us  [local(): pl.pallas_call(functools.partial(kernel, n_ep, n_tp), out_shape=jax.Shape...]
    reduce_scatter x1 -> x0, waiting for transfers between devices: 20.2 us -> none  [local(): lax.psum_scatter(lax.dot_general(down_mat, hidden, (((0,), (1,)), ((), ()...]
    all_to_all x1 -> x0, blocking collectives: 15 us -> none  [local(): lax.all_to_all(own_share, 'ep', split_axis=0, concat_axis=0, tiled=True)]
    dot_general x3 -> x0, matrix products: 11 us -> none  [the longest x1 6.54 us: local(): lax.dot_general(down_mat, hidden, (((0,), (1,)), ((), ())), preferred_ele...]
    all_gather x1 -> x0, blocking collectives: 7.82 us -> none  [local(): pieces = lax.all_gather(arrived, 'tp', axis=1, tiled=True)]
    all_to_all x1 -> x0, waiting for transfers between devices: 7.77 us -> none  [local(): back = lax.all_to_all(summed, 'ep', split_axis=1, concat_axis=1, tiled=True)]
    all_to_all x1 -> x0, starting transfers between devices: 5.5 us -> none  [local(): back = lax.all_to_all(summed, 'ep', split_axis=1, concat_axis=1, tiled=True)]
    unnamed x4 -> x3, local copies, waits for them, and re-layouts: 0.85 us -> 4.1 us
  transfers between devices with their start and end apart: 2 -> 0, of which waited for: 2 -> 0; matrix products, arithmetic and copies ran while one was open for 0% -> 0% of each run, Pallas kernels for 0% -> 0%
where the time goes in v1:
time: 36.3 us; the launch traced here: 36 us
  Pallas kernels  31.9 us (88%)
  local copies, waits for them, and re-layouts  4.1 us (11%)
    pallas_call x1, Pallas kernels, local(): pl.pallas_call(functools.partial(kernel, n_ep, n_tp), out_shape=jax.Shape...  31.9 us
    unnamed x3, local copies, waits for them, and re-layouts  4.1 us

profile of v1, /device:TPU:0, one launch (start us, length us, event | category | flops | bytes accessed | tf_op | source)
XLA Modules:
  0.0 36.0 jit_solution(13467866577021347852)
XLA Ops:
  0.0 1.4 %copy.8.route_ref = s32[24,4]{1,0:T(8,128)} copy(s32[24,4]{0,1:T(4,128)} %param.9) | data formatting | bytes 768 | tf_op args[2]
  1.4 1.4 %copy.9.weight_ref = f32[24,4]{1,0:T(8,128)} copy(f32[24,4]{0,1:T(4,128)} %param.10) | data formatting | bytes 768 | tf_op args[3]
  2.7 31.9 %shard_map.73 = bf16[24,768]{1,0:T(8,128)(2,1)} custom-call(bf16[24,3072]{1,0:T(8,128)(2,1)} %tok_ref.1, f32[1,3072]{1,0:T(1,128)} %bitcast.1, s32[24,4]{1,0:T(8,128)} %copy.8.route_ref, f32[24,4]{1,0:T(8,128)} %copy.9.weight_ref, bf16[1,3072,768]{2,1,0:T(8,128)(2,1)} %wg_hbm.1, bf16[1,3072,768]{2,1,0:T(8,128)(2,1)} %wu_hbm.1, bf16[1,768,3072]{2,1,0:T(8,128)(2,1)} %wd_hbm.1), custom_call_target="tpu_custom_call" | custom-call | tf_op jit(solution)/shard_map/pallas_call | solution.py:344
  34.6 1.4 %copy.11 = bf16[24,768]{1,0:T(8,128)(2,1)} copy(bf16[24,768]{1,0:T(8,128)(2,1)} %shard_map.73) | data formatting | bytes 73728

commit v2 on v1

--- a/solution.py
+++ b/solution.py
@@ -26,7 +26,7 @@
 def kernel(
     n_ep, n_tp, tok_ref, gain_ref, route_ref, weight_ref, wg_hbm, wu_hbm, wd_hbm, out_ref,
     wg, wu, wd, acc_g, acc_u, sbuf, gbuf, part, din, ysend, yin, own, obuf, back,
-    w_sem, a_send, a_recv, yf_send, yf_recv, cf_send, cf_recv, rl_send, rl_recv,
+    w_sem, a_send, a_recv, ag_send, ag_recv, yf_send, yf_recv, cf_send, cf_recv, rl_send, rl_recv,
     d_send, d_recv, ys_send, ys_recv, b_send, b_recv,
 ):
     me = lax.axis_index("ep")
@@ -36,9 +36,12 @@
     core = y * 2 + (1 - c)
     toks, width = tok_ref.shape
     share = width // n_tp
-    slot_rows = sbuf.shape[1]
+    slot_rows = sbuf.shape[2]
     rows = n_ep * slot_rows
-    top = route_ref.shape[1]
+    top = route_ref.shape[0]
+    group = 4 if n_ep % 4 == 0 else 1
+    base = me // group * group
+    beyond = n_ep - group
     others = [(y + d) % ny for d in range(1, ny)]
     order = [j, core] + [yy * 2 + c for yy in others] + [yy * 2 + (1 - c) for yy in others]
     aligned = share % 128 == 0
@@ -89,57 +92,62 @@
         pl.semaphore_signal(barrier, inc=1, device_id=(me, peer), device_id_type=MESH)
 
     routes = route_ref[...]
-    lanes = lax.broadcasted_iota(jnp.int32, (toks, 128), 1)
-    chosen = jnp.zeros((toks, 128), F32)
-    weights = jnp.zeros((toks, 128), F32)
+    experts = lax.broadcasted_iota(jnp.int32, (128, toks), 0)
+    chosen = jnp.zeros((128, toks), F32)
+    weights = jnp.zeros((128, toks), F32)
     for k in range(top):
-        hit = routes[:, k : k + 1] == lanes
+        hit = routes[k : k + 1, :] == experts
         chosen += jnp.where(hit, 1.0, 0.0)
-        weights += jnp.where(hit, weight_ref[:, k : k + 1], 0.0)
-    before = lax.broadcasted_iota(jnp.int32, (toks, toks), 0) > lax.broadcasted_iota(
+        weights += jnp.where(hit, weight_ref[k : k + 1, :], 0.0)
+    before = lax.broadcasted_iota(jnp.int32, (toks, toks), 0) < lax.broadcasted_iota(
         jnp.int32, (toks, toks), 1
     )
-    rank = jnp.dot(
-        jnp.where(before, 1.0, 0.0).astype(BF16), chosen.astype(BF16), preferred_element_type=F32
-    )
+    chosen = chosen.astype(BF16)
+    rank = jnp.dot(chosen, jnp.where(before, 1.0, 0.0).astype(BF16), preferred_element_type=F32)
     r_row = lax.broadcasted_iota(jnp.int32, (rows, 128), 0)
     r_exp = lax.broadcasted_iota(jnp.int32, (rows, 128), 1)
     spread = jnp.where(r_row // slot_rows == r_exp, 1.0, 0.0).astype(BF16)
-    nt = (((1,), (1,)), ((), ()))
-
-    def across(a, b):
-        return lax.dot_general(a, b, nt, preferred_element_type=F32)
-
-    slot_a = (lax.broadcasted_iota(jnp.int32, (rows, toks), 0) % slot_rows).astype(F32)
-    taken = across(spread, chosen.astype(BF16)) > 0.5
-    select = jnp.where(
-        taken & (across(spread, rank.astype(BF16)) == slot_a), 1.0, 0.0
-    ).astype(BF16)
+
+    def spread_out(a):
+        return jnp.dot(spread, a.astype(BF16), preferred_element_type=F32)
+
+    slot = (lax.broadcasted_iota(jnp.int32, (rows, toks), 0) % slot_rows).astype(F32)
+    here = (spread_out(chosen) > 0.5) & (spread_out(rank) == slot)
+    select = jnp.where(here, 1.0, 0.0).astype(BF16)
 
     values = tok_ref[...].astype(F32)
     scale = lax.rsqrt(jnp.mean(values * values, axis=-1, keepdims=True) + NORM_EPS)
 
-    def put_share(tok_part, gain_part):
+    def put_share(at, tok_part, gain_part):
         normal = (tok_part.astype(F32) * scale * gain_part).astype(BF16)
         sending = jnp.dot(select, normal, preferred_element_type=F32).astype(BF16)
-        sbuf[...] = sending.reshape(n_ep, slot_rows, share)
+        sbuf[at] = sending.reshape(n_ep, slot_rows, share)
 
     if aligned:
-        put_share(tok_ref[:, part_rows(j)], gain_ref[:, part_rows(j)])
+        for yy in [y] + others:
+            cut = part_rows(yy * 2 + c)
+            put_share(yy, tok_ref[:, cut], gain_ref[:, cut])
     else:
         for s in range(n_tp):
 
-            @pl.when(j == s)
+            @pl.when(c == s % 2)
             def _(s=s):
                 cut = slice(s * share, (s + 1) * share)
-                put_share(tok_ref[:, cut], gain_ref[:, cut])
+                put_share(s // 2, tok_ref[:, cut], gain_ref[:, cut])
 
     pl.semaphore_wait(barrier, n_ep - 1 + 1 + ny - 1)
 
     def a_copy(dst, src):
         return pltpu.make_async_remote_copy(
-            src_ref=sbuf.at[dst], dst_ref=gbuf.at[j, src], send_sem=a_send.at[dst],
+            src_ref=sbuf.at[y, dst], dst_ref=gbuf.at[j, src], send_sem=a_send.at[dst],
             recv_sem=a_recv.at[src], device_id=(dst, j), device_id_type=MESH,
+        )
+
+    def ag_copy(dst, src, yy):
+        return pltpu.make_async_remote_copy(
+            src_ref=sbuf.at[yy, dst], dst_ref=gbuf.at[yy * 2 + c, src],
+            send_sem=ag_send.at[yy, dst], recv_sem=ag_recv.at[yy, src],
+            device_id=(dst, j), device_id_type=MESH,
         )
 
     def yf_copy(block, slot, yy, frm):
@@ -162,32 +170,37 @@
             recv_sem=rl_recv.at[frm], device_id=(me, core), device_id_type=MESH,
         )
 
-    each(n_ep - 1, lambda k: a_copy((me + far(k)) % n_ep, me).start())
-    gbuf[j, me] = sbuf[me]
-
-    def forward(block):
+    def outer(k):
+        return (base + group + (me - base + k) % beyond) % n_ep
+
+    near = [base + (me - base + d) % group for d in range(1, group)]
+    if beyond:
+        each(beyond, lambda k: a_copy(outer(k), me).start())
+    for dst in near:
+        a_copy(dst, me).start()
+    for yy in others:
+        for dst in near:
+            ag_copy(dst, me, yy).start()
+    for yy in [y] + others:
+        gbuf[yy * 2 + c, me] = sbuf[yy, me]
+    cf_copy(me, j).start()
+
+    def arrive(k):
+        src = outer(k)
+        a_copy(src, src).wait_recv()
         for yy in others:
-            yf_copy(block, j, yy, y).start()
-        cf_copy(block, j).start()
-
-    forward(me)
-
-    def arrive(k):
-        src = (me + far(n_ep - 2 - k)) % n_ep
+            yf_copy(src, j, yy, y).start()
+        cf_copy(src, j).start()
+
+    if beyond:
+        each(beyond, arrive)
+    for src in near:
         a_copy(src, src).wait_recv()
-        forward(src)
-
-    each(n_ep - 1, arrive)
-
-    place = across(weights.astype(BF16), spread)
-    rest = weights - weights.astype(BF16).astype(F32)
-    rest_place = across(rest.astype(BF16), spread)
-    slot_b = (lax.broadcasted_iota(jnp.int32, (toks, rows), 1) % slot_rows).astype(F32)
-    here = (across(rank.astype(BF16), spread) == slot_b) & (
-        across(chosen.astype(BF16), spread) > 0.5
-    )
-    mix_high = jnp.where(here, place, 0.0).astype(BF16)
-    mix_low = jnp.where(here, rest_place, 0.0).astype(BF16)
+        cf_copy(src, j).start()
+
+    high = weights.astype(BF16)
+    mix_high = jnp.where(here, spread_out(high), 0.0).astype(BF16)
+    mix_low = jnp.where(here, spread_out(weights - high.astype(F32)), 0.0).astype(BF16)
 
     def project(at):
         s = order[at]
@@ -208,9 +221,11 @@
 
     project(0)
     for yy in others:
-        slot = yy * 2 + c
-        each(n_ep, lambda b: yf_copy(b, slot, yy, yy).wait_recv())
-        rl_copy(slot, yy).start()
+        for src in near:
+            ag_copy(src, src, yy).wait_recv()
+        if beyond:
+            each(beyond, lambda k: yf_copy(outer(k), yy * 2 + c, yy, yy).wait_recv())
+        rl_copy(yy * 2 + c, yy).start()
     each(n_ep, lambda b: cf_copy(b, core).wait_recv())
     project(1)
     for at in range(2, 1 + ny):
@@ -305,8 +320,9 @@
     back[me] = value
     each(n_ep - 1, lambda k: b_copy((me + k + 1) % n_ep, (me + k + 1) % n_ep).wait_recv())
     returned = back[...].reshape(rows, share)
-    mixed = jnp.dot(mix_high, returned, preferred_element_type=F32)
-    mixed += jnp.dot(mix_low, returned, preferred_element_type=F32)
+    over_rows = (((0,), (0,)), ((), ()))
+    mixed = lax.dot_general(mix_high, returned, over_rows, preferred_element_type=F32)
+    mixed += lax.dot_general(mix_low, returned, over_rows, preferred_element_type=F32)
     out_ref[...] = mixed.astype(BF16)
 
     def drain(k):
@@ -319,10 +335,14 @@
     def drain_blocks(b):
         cf_copy(b, j).wait_send()
         for yy in others:
-            yf_copy(b, j, yy, y).wait_send()
             ys_copy(b, yy, y).wait_send()
 
     each(n_ep, drain_blocks)
+    for yy in others:
+        if beyond:
+            each(beyond, lambda k: yf_copy(outer(k), j, yy, y).wait_send())
+        for dst in near:
+            ag_copy(dst, me, yy).wait_send()
     for yy in others:
         rl_copy(yy * 2 + c, yy).wait_send()
     for yy in others + [y]:
@@ -352,7 +372,7 @@
             pltpu.VMEM((hidden, width), BF16),
             pltpu.VMEM((rows, hidden), F32),
             pltpu.VMEM((rows, hidden), F32),
-            pltpu.VMEM(blocks, BF16),
+            pltpu.VMEM((ny,) + blocks, BF16),
             pltpu.VMEM((n_tp,) + blocks, BF16),
             pltpu.VMEM((ny,) + blocks, BF16),
             pltpu.VMEM((ny,) + blocks, BF16),
@@ -363,6 +383,7 @@
             pltpu.VMEM(blocks, BF16),
             dma((3, n_tp)),
             dma((n_ep,)), dma((n_ep,)),
+            dma((ny, n_ep)), dma((ny, n_ep)),
             dma((ny, n_ep)), dma((ny, n_ep)),
             dma((n_ep,)), dma((n_ep,)),
             dma((ny,)), dma((ny,)),
@@ -371,7 +392,7 @@
             dma((n_ep,)), dma((n_ep,)),
         ],
         compiler_params=pltpu.CompilerParams(collective_id=0, has_side_effects=True),
-    )(tokens, norm_gain.reshape(1, width), routing, route_weight, w_gate, w_up, w_down)
+    )(tokens, norm_gain.reshape(1, width), routing.T, route_weight.T, w_gate, w_up, w_down)
 
 
 def solution(mesh):

time: 36.3 us -> 33.1 us (0.912)
  local copies, waits for them, and re-layouts: 4.1 us -> 1.39 us
  Pallas kernels: 31.9 us -> 31.5 us
    unnamed x3 -> x1, local copies, waits for them, and re-layouts: 4.1 us -> 1.39 us
    pallas_call x1, Pallas kernels: 31.9 us -> 31.5 us  [local(): pl.pallas_call(functools.partial(kernel, n_ep, n_tp), out_shape=jax.Shape...]
where the time goes in v2:
time: 33.1 us; the launch traced here: 32.9 us
  Pallas kernels  31.5 us (95%)
  local copies, waits for them, and re-layouts  1.39 us (4%)
    pallas_call x1, Pallas kernels, local(): pl.pallas_call(functools.partial(kernel, n_ep, n_tp), out_shape=jax.Shape...  31.5 us
    unnamed x1, local copies, waits for them, and re-layouts  1.39 us

profile of v2, /device:TPU:0, one launch (start us, length us, event | category | flops | bytes accessed | tf_op | source)
XLA Modules:
  0.0 32.9 jit_solution(16292836320182589687)
XLA Ops:
  0.0 31.5 %shard_map.73 = bf16[24,768]{1,0:T(8,128)(2,1)} custom-call(bf16[24,3072]{1,0:T(8,128)(2,1)} %tok_ref.1, f32[1,3072]{1,0:T(1,128)} %bitcast.3, s32[4,24]{1,0:T(4,128)} %bitcast.4, f32[4,24]{1,0:T(4,128)} %bitcast.5, bf16[1,3072,768]{2,1,0:T(8,128)(2,1)} %wg_hbm.1, bf16[1,3072,768]{2,1,0:T(8,128)(2,1)} %wu_hbm.1, bf16[1,768,3072]{2,1,0:T(8,128)(2,1)} %wd_hbm.1), custom_call_target="tpu_custom_call" | custom-call | tf_op jit(solution)/shard_map/pallas_call | solution.py:364
  31.5 1.4 %copy.9 = bf16[24,768]{1,0:T(8,128)(2,1)} copy(bf16[24,768]{1,0:T(8,128)(2,1)} %shard_map.73) | data formatting | bytes 73728
